TPU v7x, 32 devices: a whole 2x2x4 slice. The times are simulated.
32 devices in a mesh: sp: 4 (over y, x), tp: 8 (over z, core).
Axes of the slice: x: 2, y: 2, z: 4, core: 2. Of those that a mesh axis runs over, the one named last changes fastest.
Arguments:
- queries: bfloat16 [1536, 2048], P('sp', 'tp'), may hold values from -6 to 6
- keys: bfloat16 [1536, 2048], P('sp', 'tp'), may hold values from -6 to 6
- values: bfloat16 [1536, 2048], P('sp', 'tp'), may hold values from -6 to 6
- key_bias: bfloat16 [1536, 32], P('sp', 'tp'), may hold values from -16 to 0
- head_gain: float32 [32, 64], P('tp'), may hold values from 0.1 to 1.9
- out_weight: bfloat16 [2048, 2048], P('tp'), may hold values from -0.125 to 0.125
- residual: bfloat16 [1536, 2048], P(('sp', 'tp')), may hold values from -6 to 6
- norm_gain: float32 [2048], replicated, may hold values from 0.1 to 1.9
- gate_proj: bfloat16 [4, 2048, 7168], P('sp', None, 'tp'), may hold values from -0.125 to 0.125
- up_proj: bfloat16 [4, 2048, 7168], P('sp', None, 'tp'), may hold values from -0.125 to 0.125
- down_proj: bfloat16 [4, 7168, 2048], P('sp', 'tp'), may hold values from -0.0625 to 0.0625
- expert_choice: int32 [1536, 2], P(('sp', 'tp')), may hold values from 0 to 3, all different within a row; in each aligned block of 48 rows (0 to 47, 48 to 95, ...) at most 48 rows name the same one
- expert_weights: float32 [1536, 2], P(('sp', 'tp')), may hold values from 0.2 to 1
Outputs:
- layer_out: bfloat16 [1536, 2048], P(('sp', 'tp'))
Inputs may be any that keep to these rules, and one draw needn't show every extreme that they name: `expert_choice`: in each aligned block of 48 rows (the rows of one device), no expert is named more than 48 times; the two experts of a row differ.
All inputs are finite; a program needn't handle non-finite values.
Results may differ from a plain program's by a relative error of at most 0.019.
Values may be sent and summed in bfloat16 or wider, within the bound.
A program may use at most 128 MiB of HBM per device.

v0:
```python
import jax
import jax.numpy as jnp
from jax import lax
from jax.sharding import PartitionSpec as P

epsilon = 1e-06


def rms_scaled(values_in):
    return values_in * lax.rsqrt(jnp.mean(values_in * values_in, axis=-1, keepdims=True) + epsilon)


def expert_partial(row_block, gate_matrix, up_matrix, down_matrix):
    gate_part = jnp.dot(row_block, gate_matrix, preferred_element_type=jnp.float32)
    up_part = jnp.dot(row_block, up_matrix, preferred_element_type=jnp.float32)
    hidden = (jax.nn.silu(gate_part) * up_part).astype(jnp.bfloat16)
    return jnp.dot(hidden, down_matrix, preferred_element_type=jnp.float32)


def choice_ranks(routes, experts_all):
    flat_routes = routes.reshape(routes.shape[:-2] + (-1,))
    onehot = (flat_routes[..., None] == jnp.arange(experts_all, dtype=jnp.int32)).astype(jnp.int32)
    before = jnp.cumsum(onehot, axis=-2) - onehot
    return jnp.sum(before * onehot, axis=-1).reshape(routes.shape)


def slot_tokens(slot_index, targets, missing):
    flat_slots = slot_index.reshape(-1)
    owners = jnp.arange(flat_slots.shape[0], dtype=jnp.int32) // 2
    matches = flat_slots[None, :] == jnp.arange(targets, dtype=jnp.int32)[:, None]
    owner_found = jnp.sum(jnp.where(matches, owners[None, :], 0), axis=1)
    return jnp.where(jnp.any(matches, axis=1), owner_found, missing)


def on_device(
    queries,
    keys,
    values,
    key_bias,
    head_gain,
    out_weight,
    residual,
    norm_gain,
    gate_proj,
    up_proj,
    down_proj,
    expert_choice,
    expert_weights,
):
    rows_own = queries.shape[0]
    heads_here = head_gain.shape[0]
    head_size = head_gain.shape[1]
    model_width = out_weight.shape[1]
    seq_devices = lax.axis_size("sp")
    head_devices = lax.axis_size("tp")
    own_start = lax.axis_index("sp") * rows_own
    query_pos = own_start + jnp.arange(rows_own, dtype=jnp.int32)
    query_heads = queries.reshape(rows_own, heads_here, head_size)

    def key_block(slot_state, key_rows, value_rows, bias_rows, key_start):
        key_heads = key_rows.reshape(rows_own, heads_here, head_size)
        value_heads = value_rows.reshape(rows_own, heads_here, head_size)
        scores = jnp.einsum(
            "qhd,khd->hqk", query_heads, key_heads, preferred_element_type=jnp.float32
        ) * head_size ** (-0.5)
        scores = scores + bias_rows.astype(jnp.float32).T[:, None, :]
        key_pos = key_start + jnp.arange(rows_own, dtype=jnp.int32)
        earlier = (key_pos[None, :] < query_pos[:, None])[None, :, :]
        log_drops = jnp.where(earlier, jax.nn.log_sigmoid(-scores), 0.0)
        suffix = lax.cumsum(log_drops, axis=2, reverse=True) - log_drops
        within = jnp.where(earlier, jnp.exp(jax.nn.log_sigmoid(scores) + suffix), 0.0).astype(
            jnp.bfloat16
        )
        block_part = jnp.einsum(
            "hqk,khd->qhd", within, value_heads, preferred_element_type=jnp.float32
        )
        block_index = key_start // rows_own
        sums_new = lax.dynamic_update_index_in_dim(
            slot_state[0], block_part.reshape(rows_own, heads_here * head_size), block_index, 0
        )
        totals_new = lax.dynamic_update_index_in_dim(
            slot_state[1], jnp.sum(log_drops, axis=2), block_index, 0
        )
        return (sums_new, totals_new)

    empty_state = (
        jnp.zeros((seq_devices, rows_own, heads_here * head_size), jnp.float32),
        jnp.zeros((seq_devices, heads_here, rows_own), jnp.float32),
    )
    key_piece = lax.all_gather(keys, "sp", axis=0, tiled=True)
    value_piece = lax.all_gather(values, "sp", axis=0, tiled=True)
    bias_piece = lax.all_gather(key_bias, "sp", axis=0, tiled=True)

    def visit(block_count, state_in):
        offset = block_count * rows_own

        def take_rows(array):
            return lax.dynamic_slice_in_dim(array, offset, rows_own, 0)

        def compute(state_now):
            return key_block(
                state_now,
                take_rows(key_piece),
                take_rows(value_piece),
                take_rows(bias_piece),
                offset,
            )

        def keep(state_now):
            return state_now

        return lax.cond(offset <= own_start, compute, keep, state_in)

    block_sums, totals = lax.fori_loop(0, key_piece.shape[0] // rows_own, visit, empty_state)
    carried = jnp.sum(totals, axis=0, keepdims=True) - jnp.cumsum(totals, axis=0)
    factors = jnp.exp(carried).transpose(0, 2, 1)[..., None]
    mixture = jnp.sum(
        factors * block_sums.reshape(seq_devices, rows_own, heads_here, head_size), axis=0
    )
    attended = (
        (rms_scaled(mixture) * head_gain)
        .astype(jnp.bfloat16)
        .reshape(rows_own, heads_here * head_size)
    )
    row_share = rows_own // head_devices
    merged = lax.all_to_all(attended, "tp", split_axis=0, concat_axis=1, tiled=True)
    projected = jnp.dot(
        merged,
        lax.all_gather(out_weight, "tp", axis=0, tiled=True),
        preferred_element_type=jnp.float32,
    )
    stream = (residual.astype(jnp.float32) + projected).astype(jnp.bfloat16)
    normed = (rms_scaled(stream.astype(jnp.float32)) * norm_gain).astype(jnp.bfloat16)
    local_experts = gate_proj.shape[0]
    experts_all = local_experts * seq_devices
    capacity = 4 * rows_own // (head_devices * experts_all)
    own_slots = expert_choice * capacity + choice_ranks(expert_choice, experts_all)
    wanted = slot_tokens(own_slots, experts_all * capacity, row_share)
    outgoing = jnp.take(normed, wanted, axis=0, mode="fill", fill_value=0)
    arrived = lax.all_to_all(
        outgoing.reshape(seq_devices, local_experts, capacity, model_width),
        "sp",
        split_axis=0,
        concat_axis=0,
        tiled=True,
    )
    row_piece = lax.all_gather(arrived, "tp", axis=0, tiled=True)
    count_rows = row_piece.shape[0]
    partials = jnp.stack(
        [
            expert_partial(
                row_piece[:, 0].reshape(-1, model_width), gate_proj[0], up_proj[0], down_proj[0]
            ).reshape(count_rows, capacity, model_width)
        ],
        axis=1,
    )
    summed = lax.psum_scatter(partials.astype(jnp.bfloat16), "tp", scatter_dimension=0, tiled=True)
    returned = lax.all_to_all(summed, "sp", split_axis=0, concat_axis=0, tiled=True).reshape(
        experts_all * capacity, model_width
    )
    picked = jnp.take(returned, own_slots, axis=0).astype(jnp.float32)
    combined = jnp.sum(expert_weights[:, :, None] * picked, axis=1)
    return (stream.astype(jnp.float32) + combined).astype(jnp.bfloat16)


def solution(mesh):
    placed = (
        P("sp", "tp"),
        P("sp", "tp"),
        P("sp", "tp"),
        P("sp", "tp"),
        P("tp", None),
        P("tp", None),
        P(("sp", "tp"), None),
        P(),
        P("sp", None, "tp"),
        P("sp", None, "tp"),
        P("sp", "tp", None),
        P(("sp", "tp"), None),
        P(("sp", "tp"), None),
    )
    return jax.shard_map(
        on_device, mesh=mesh, in_specs=placed, out_specs=P(("sp", "tp"), None), check_vma=False
    )
```

profile of v0, /device:TPU:0, one launch (start us, length us, event | category | flops | bytes accessed | tf_op | source)
XLA Modules:
  0.0 380.5 jit_solution(13210839301603181166)
XLA Ops:
  9.4 1.7 copy.83
  11.2 11.0 %all_gather.17 = bf16[1536,4]{0,1:T(4,128)(2,1)} all-gather(bf16[384,4]{0,1:T(4,128)(2,1)} %param.20), channel_id=1, replica_groups=mesh['sp'=4,'tp'=8] {'sp'}, dimensions={0}, use_global_device_ids=true | all-gather | bytes 15360 | tf_op jit(solution)/shard_map/all_gather | solution.py:92
  22.2 12.4 %all_gather.15 = bf16[1536,256]{0,1:T(8,128)(2,1)} all-gather(bf16[384,256]{0,1:T(8,128)(2,1)S(1)} %copy.81), channel_id=1, replica_groups=mesh['sp'=4,'tp'=8] {'sp'}, dimensions={0}, use_global_device_ids=true | all-gather | bytes 983040 | tf_op jit(solution)/shard_map/all_gather | solution.py:91
  34.5 13.4 %all_gather.16 = bf16[1536,256]{0,1:T(8,128)(2,1)} all-gather(bf16[384,256]{0,1:T(8,128)(2,1)S(1)} %copy.82), channel_id=1, replica_groups=mesh['sp'=4,'tp'=8] {'sp'}, dimensions={0}, use_global_device_ids=true | all-gather | bytes 983040 | tf_op jit(solution)/shard_map/all_gather | solution.py:90
  47.9 1.3 broadcast_in_dim.84
  49.8 28.2 %while.17 = (s32[]{:T(128)}, f32[4,384,256]{1,2,0:T(8,128)}, f32[4,4,384]{2,1,0:T(4,128)}, s32[]{:T(128)}, bf16[1536,256]{0,1:T(8,128)(2,1)}, /*index=5*/bf16[15...) while((s32[]{:T(128)}, f32[4,384,256]{1,2,0:T(8,128)}, ...), condition=%wide.region_6.7_spmd.clone.clone, body=%wide.region_0.6_spmd.clone.clone.sunk | while | flops 246117120 | bytes 38572464 | solution.py:114
  49.8 28.0 %conditional.4 = ((f32[4,384,256]{1,2,0:T(8,128)}, f32[4,4,384]{2,1,0:T(4,128)})) conditional(s32[]{:T(128)} %convert_element_type.76, (f32[4,384,256]{1,2,0:T(8,128)}, f32[4,4,384]{2,1,0:T(4,128)}) %tuple.53, (s32[]{:T(128)}, bf16[1536,256]{0,1:T(8,128)(2,1)}, s32[]{:T(128)}, bf16[1536,256]{0,1:T(8,128)(2,1)}, bf16[384,4,64]{0,2,1:T(8,128)(2,1)}, ...), branch_computations={%region_1.0_spmd, %region_2.5_spmd} | conditional | flops 246117120 | bytes 38570716 | solution.py:112
  51.7 4.3 %fusion.15 = (f32[4,384]{1,0:T(4,128)S(1)}, f32[4,384,384]{1,2,0:T(8,128)S(1)}, f32[4,384,384]{2,1,0:T(8,128)}) fusion(f32[4,384]{1,0:T(4,128)S(1)} %convert_bitcast_fusion, pred[384,384]{0,1:T(8,128)(4,1)S(1)} %broadcast_compare_fusion, bf16[384,4,64]{0,2,1:T(8,128)(2,1)S(1)} %bitcast.92, bf16[384,4,64]{0,2,1:T(8,128)(2,1)} %get-tuple-element.177), kind=kOutput, calls=%fused_computation.33 | convolution fusion | flops 81984000 | bytes 5271552 | tf_op jit(solution)/shard_map/while/body/eval_jaxpr/cond/branch_1_fun/qhd,khd->hqk/dot_general | solution.py:63
  56.0 14.0 %fusion.2 = f32[4,384,3,128]{1,2,3,0:T(4,128)S(1)} fusion(f32[4,384,3,128]{1,3,2,0:T(8,128)S(1)} %bitcast.88), kind=kOutput, calls=%fused_computation.5 | output fusion | flops 74907648 | bytes 4718592 | tf_op jit(solution)/shard_map/reduce-window
  70.9 1.5 copy-done
  72.3 3.6 fusion.8
  79.5 1.6 fusion.22
  83.2 4.8 %all-to-all-start = ((bf16[8,48,256]{2,1,0:T(8,128)(2,1)}), bf16[8,48,256]{2,1,0:T(8,128)(2,1)S(1)}, u32[]{:S(2)}, u32[]{:S(2)}) async-start(bf16[8,48,256]{2,1,0:T(8,128)(2,1)} %multiply_convert_fusion.2), calls=%async_computation | async-start | bytes 393216 | tf_op jit(solution)/shard_map/all_to_all | solution.py:126
  89.5 6.8 %all-to-all-done = bf16[8,48,256]{2,1,0:T(8,128)(2,1)S(1)} async-done(((bf16[8,48,256]{2,1,0:T(8,128)(2,1)}), bf16[8,48,256]{2,1,0:T(8,128)(2,1)S(1)}, u32[]{:S(2)}, u32[]{:S(2)}) %all-to-all-start) | async-done | bytes 196640 | tf_op jit(solution)/shard_map/all_to_all | solution.py:126
  96.4 5.1 %multiply_reduce_fusion.1 = (f32[48]{0:T(128)S(1)}, f32[48,2048]{1,0:T(8,128)S(1)}) fusion(bf16[48,2048]{1,0:T(8,128)(2,1)S(1)} %bitcast.94, bf16[2048,2048]{1,0:T(8,128)(2,1)} %all-gather.3.cloned.1.call-done, bf16[48,2048]{1,0:T(8,128)(2,1)S(1)} %copy-done.1), kind=kOutput, calls=%fused_computation.54 | convolution fusion | flops 403242944 | bytes 9175232 | tf_op jit(solution)/shard_map/dot_general | solution.py:127
  102.9 96.4 %all_to_all.26 = bf16[4,1,48,2048]{3,2,1,0:T(8,128)(2,1)} all-to-all(bf16[4,1,48,2048]{3,2,1,0:T(8,128)(2,1)S(1)} %broadcast_select_fusion), channel_id=1, replica_groups=mesh['sp'=4,'tp'=8] {'sp'}, dimensions={0} | all-to-all | bytes 1572864 | tf_op jit(solution)/shard_map/all_to_all | solution.py:140
  199.4 63.5 %all-gather.5.cloned.1.call-done = bf16[32,1,48,2048]{3,2,1,0:T(8,128)(2,1)} async-done(((bf16[4,1,48,2048]{3,2,1,0:T(8,128)(2,1)}), bf16[32,1,48,2048]{3,2,1,0:T(8,128)(2,1)}) %all-gather.5.cloned.1.call-update) | async-done | bytes 6291472 | tf_op jit(solution)/shard_map/all_gather | solution.py:147
  262.9 10.0 %fusion.18 = f32[1536,896]{1,0:T(8,128)S(1)} fusion(bf16[1536,2048]{1,0:T(8,128)(2,1)} %bitcast.101, bf16[1,2048,896]{2,1,0:T(8,128)(2,1)} %param.25), kind=kOutput, calls=%fused_computation.38 | convolution fusion | flops 5637144576 | bytes 15466496 | tf_op jit(solution)/shard_map/dot_general | solution.py:14
  272.9 7.1 %multiply_convert_fusion = bf16[1536,896]{1,0:T(8,128)(2,1)S(1)} fusion(f32[1536,896]{1,0:T(8,128)S(1)} %fusion.18, bf16[1536,2048]{1,0:T(8,128)(2,1)S(1)} %bitcast.102, bf16[1,2048,896]{2,1,0:T(8,128)(2,1)S(1)} %copy-done.7), kind=kOutput, calls=%fused_computation.35 | convolution fusion | flops 5645402112 | bytes 18219008 | tf_op jit(solution)/shard_map/dot_general | solution.py:15
  280.0 8.7 %convert_bitcast_fusion.1 = bf16[32,1,48,2048]{3,2,0,1:T(8,128)(2,1)} fusion(bf16[32,48,896]{2,1,0:T(8,128)(2,1)S(1)} %bitcast.103, bf16[1,896,2048]{2,1,0:T(8,128)(2,1)S(1)} %copy-done.8), kind=kOutput, calls=%fused_computation.34 | convolution fusion | flops 5640290304 | bytes 12713984 | tf_op jit(solution)/shard_map/dot_general | solution.py:17
  288.8 68.5 %reduce-scatter.2.cloned.1.call-done = bf16[4,1,48,2048]{3,2,0,1:T(8,128)(2,1)} async-done(((bf16[32,1,48,2048]{3,2,0,1:T(8,128)(2,1)}), bf16[4,1,48,2048]{3,2,0,1:T(8,128)(2,1)}) %reduce-scatter.2.cloned.1.call-update) | async-done | bytes 786448 | tf_op jit(solution)/shard_map/reduce_scatter | solution.py:157
  357.3 3.7 all-to-all-start.2
  361.5 8.6 %all-to-all-done.2 = bf16[4,1,48,2048]{3,2,1,0:T(8,128)(2,1)S(1)} async-done(((bf16[4,1,48,2048]{3,2,1,0:T(8,128)(2,1)}), bf16[4,1,48,2048]{3,2,1,0:T(8,128)(2,1)S(1)}, u32[]{:S(2)}, u32[]{:S(2)}) %all-to-all-start.2) | async-done | bytes 786464 | tf_op jit(solution)/shard_map/all_to_all | solution.py:158
  371.2 2.1 multiply_reduce_fusion
  (88 shorter events, 16.8 us)
Async XLA Ops:
  6.5 89.9 %all-gather.3.cloned.1.call-start = ((), (), s32[]{:S(2)}) async-start(), calls=%async_computation.4 | async-start | bytes 9437184 | tf_op jit(solution)/shard_map/all_gather | solution.py:129
  70.6 1.7 copy-start
  79.5 2.9 copy-start.4
  81.1 7.0 %copy-start.3 = (s32[48,2]{0,1:T(2,128)S(1)}, s32[48,2]{0,1:T(2,128)}, u32[]{:S(2)}) copy-start(s32[48,2]{0,1:T(2,128)} %param.28) | copy-start | bytes 1156
  81.3 15.1 %copy-start.1 = (bf16[48,2048]{1,0:T(8,128)(2,1)S(1)}, bf16[48,2048]{1,0:T(8,128)(2,1)}, u32[]{:S(2)}) copy-start(bf16[48,2048]{1,0:T(8,128)(2,1)} %param.23) | copy-start | bytes 589828
  83.2 13.1 %all-to-all-start = ((bf16[8,48,256]{2,1,0:T(8,128)(2,1)}), bf16[8,48,256]{2,1,0:T(8,128)(2,1)S(1)}, u32[]{:S(2)}, u32[]{:S(2)}) async-start(bf16[8,48,256]{2,1,0:T(8,128)(2,1)} %multiply_convert_fusion.2), calls=%async_computation | async-start | bytes 393216 | tf_op jit(solution)/shard_map/all_to_all | solution.py:126
  88.0 174.9 %all-gather.5.cloned.1.call-start = ((), (), s32[]{:S(2)}) async-start(), calls=%async_computation.5 | async-start | bytes 7077888 | tf_op jit(solution)/shard_map/all_gather | solution.py:147
  96.4 5.1 %copy-start.2 = (f32[2048]{0:T(1024)S(1)}, f32[2048]{0:T(1024)}, u32[]{:S(2)}) copy-start(f32[2048]{0:T(1024)} %param.24) | copy-start | bytes 24580
  199.3 158.0 %reduce-scatter.2.cloned.1.call-start = ((), (), s32[]{:S(2)}) async-start(), calls=%async_computation.6 | async-start | bytes 7077888 | tf_op jit(solution)/shard_map/reduce_scatter | solution.py:157
  262.9 10.0 %copy-start.6 = (bf16[32,1,48,2048]{3,2,1,0:T(8,128)(2,1)S(1)}, bf16[32,1,48,2048]{3,2,1,0:T(8,128)(2,1)}, u32[]{:S(2)}) copy-start(bf16[32,1,48,2048]{3,2,1,0:T(8,128)(2,1)} %all-gather.5.cloned.1.call-done) | copy-start | bytes 18874372
  262.9 10.0 %copy-start.7 = (bf16[1,2048,896]{2,1,0:T(8,128)(2,1)S(1)}, bf16[1,2048,896]{2,1,0:T(8,128)(2,1)}, u32[]{:S(2)}) copy-start(bf16[1,2048,896]{2,1,0:T(8,128)(2,1)} %param.26) | copy-start | bytes 11010052
  272.9 7.1 %copy-start.8 = (bf16[1,896,2048]{2,1,0:T(8,128)(2,1)S(1)}, bf16[1,896,2048]{2,1,0:T(8,128)(2,1)}, u32[]{:S(2)}) copy-start(bf16[1,896,2048]{2,1,0:T(8,128)(2,1)} %param.27) | copy-start | bytes 11010052
  288.8 72.6 %copy-start.5 = (f32[48,2]{0,1:T(2,128)S(1)}, f32[48,2]{0,1:T(2,128)}, u32[]{:S(2)}) copy-start(f32[48,2]{0,1:T(2,128)} %param.29) | copy-start | bytes 1156
  357.3 12.7 %all-to-all-start.2 = ((bf16[4,1,48,2048]{3,2,1,0:T(8,128)(2,1)}), bf16[4,1,48,2048]{3,2,1,0:T(8,128)(2,1)S(1)}, u32[]{:S(2)}, u32[]{:S(2)}) async-start(bf16[4,1,48,2048]{3,2,1,0:T(8,128)(2,1)} %bitcast.96), calls=%async_computation.3 | async-start | bytes 1572864 | tf_op jit(solution)/shard_map/all_to_all | solution.py:158
Sparse Core Ops, SparseCore 0:
  8.9 84.8 all-gather.2
  199.4 63.4 all-gather.4
  288.9 68.3 reduce-scatter.1
where the time goes:
time: 382 us; the launch traced here: 380 us
  waiting for transfers between devices  148 us (39%)
  blocking collectives  133 us (35%)
  matrix products  35.5 us (9%)
  other arithmetic  26.7 us (7%)
  local copies, waits for them, and re-layouts  14.7 us (4%)
  between operations  13.4 us (4%)
  starting transfers between devices  8.62 us (2%)
    all_to_all x1, blocking collectives, on_device(): lax.all_to_all(outgoing.reshape(seq_devices, local_experts, capacity, mod...  96.4 us
    reduce_scatter x1, waiting for transfers between devices, on_device(): lax.psum_scatter(partials.astype(jnp.bfloat16), 'tp', scatter_dimension=0...  68.5 us
    all_gather x1, waiting for transfers between devices, on_device(): row_piece = lax.all_gather(arrived, 'tp', axis=0, tiled=True)  63.5 us
    another operation x2, other arithmetic  14.1 us
    all_gather x1, blocking collectives, on_device(): key_piece = lax.all_gather(keys, 'sp', axis=0, tiled=True)  13.4 us
    all_gather x1, blocking collectives, on_device(): value_piece = lax.all_gather(values, 'sp', axis=0, tiled=True)  12.4 us
    all_gather x1, blocking collectives, on_device(): bias_piece = lax.all_gather(key_bias, 'sp', axis=0, tiled=True)  11 us
    dot_general x1, matrix products, expert_partial(): jnp.dot(row_block, gate_matrix, preferred_element_type=jnp.float32)  9.96 us
  transfers between devices with their start and end apart: 5, of which 4 were waited for; matrix products, arithmetic and copies ran while one was open for 10% of the time, Pallas kernels for 0%

commit v1 on v0

--- a/solution.py
+++ b/solution.py
@@ -88,8 +88,11 @@
         jnp.zeros((seq_devices, heads_here, rows_own), jnp.float32),
     )
     key_piece = lax.all_gather(keys, "sp", axis=0, tiled=True)
-    value_piece = lax.all_gather(values, "sp", axis=0, tiled=True)
-    bias_piece = lax.all_gather(key_bias, "sp", axis=0, tiled=True)
+    value_piece, bias_piece = jnp.split(
+        lax.all_gather(jnp.concatenate([values, key_bias], axis=1), "sp", axis=0, tiled=True),
+        [values.shape[1]],
+        axis=1,
+    )
 
     def visit(block_count, state_in):
         offset = block_count * rows_own

time: 382 us -> 373 us (0.976)
  blocking collectives: 133 us -> 115 us
  waiting for transfers between devices: 148 us -> 158 us
    all_to_all x1, blocking collectives: 96.4 us -> 86.9 us  [on_device(): lax.all_to_all(outgoing.reshape(seq_devices, local_experts, capacity, mod...]
    all_gather x2 -> x1, blocking collectives: 23.3 us -> 15.2 us  [on_device(): lax.all_gather(jnp.concatenate([values, key_bias], axis=1), 'sp', axis=0,...]
    all_to_all x1, waiting for transfers between devices: 6.81 us -> 12.2 us  [on_device(): lax.all_to_all(attended, 'tp', split_axis=0, concat_axis=1, tiled=True)]
    all_gather x1, waiting for transfers between devices: 0.02 us -> 4.22 us  [on_device(): lax.all_gather(out_weight, 'tp', axis=0, tiled=True)]
  transfers between devices with their start and end apart: 5 -> 5, of which waited for: 4 -> 5; matrix products, arithmetic and copies ran while one was open for 10% -> 11% of each run, Pallas kernels for 0% -> 0%
where the time goes in v1:
time: 373 us; the launch traced here: 372 us
  waiting for transfers between devices  158 us (42%)
  blocking collectives  115 us (31%)
  matrix products  35.5 us (10%)
  other arithmetic  27.4 us (7%)
  local copies, waits for them, and re-layouts  14.4 us (4%)
  between operations  13.4 us (4%)
  starting transfers between devices  8.53 us (2%)
    all_to_all x1, blocking collectives, on_device(): lax.all_to_all(outgoing.reshape(seq_devices, local_experts, capacity, mod...  86.9 us
    reduce_scatter x1, waiting for transfers between devices, on_device(): lax.psum_scatter(partials.astype(jnp.bfloat16), 'tp', scatter_dimension=0...  68.5 us
    all_gather x1, waiting for transfers between devices, on_device(): row_piece = lax.all_gather(arrived, 'tp', axis=0, tiled=True)  63.5 us
    all_gather x1, blocking collectives, on_device(): lax.all_gather(jnp.concatenate([values, key_bias], axis=1), 'sp', axis=0,...  15.2 us
    another operation x2, other arithmetic  14.1 us
    all_gather x1, blocking collectives, on_device(): key_piece = lax.all_gather(keys, 'sp', axis=0, tiled=True)  13 us
    all_to_all x1, waiting for transfers between devices, on_device(): lax.all_to_all(attended, 'tp', split_axis=0, concat_axis=1, tiled=True)  12.2 us
    dot_general x1, matrix products, expert_partial(): jnp.dot(row_block, gate_matrix, preferred_element_type=jnp.float32)  9.96 us
  transfers between devices with their start and end apart: 5, of which 5 were waited for; matrix products, arithmetic and copies ran while one was open for 11% of the time, Pallas kernels for 0%

profile of v1, /device:TPU:0, one launch (start us, length us, event | category | flops | bytes accessed | tf_op | source)
XLA Modules:
  0.0 372.5 jit_solution(1242301515541195652)
XLA Ops:
  9.1 15.2 %all_gather.12 = bf16[1536,260]{0,1:T(8,128)(2,1)S(1)} all-gather(bf16[384,260]{0,1:T(8,128)(2,1)S(1)} %pad_maximum_fusion), channel_id=1, replica_groups=mesh['sp'=4,'tp'=8] {'sp'}, dimensions={0}, use_global_device_ids=true | all-gather | bytes 998400 | tf_op jit(solution)/shard_map/all_gather | solution.py:92
  26.9 13.0 %all_gather.13 = bf16[1536,256]{0,1:T(8,128)(2,1)} all-gather(bf16[384,256]{0,1:T(8,128)(2,1)S(1)} %copy.82), channel_id=1, replica_groups=mesh['sp'=4,'tp'=8] {'sp'}, dimensions={0}, use_global_device_ids=true | all-gather | bytes 983040 | tf_op jit(solution)/shard_map/all_gather | solution.py:90
  39.9 1.3 broadcast_in_dim.84
  41.8 28.1 %while.17 = (s32[]{:T(128)}, f32[4,384,256]{1,2,0:T(8,128)}, f32[4,4,384]{2,1,0:T(4,128)}, s32[]{:T(128)}, bf16[1536,256]{0,1:T(8,128)(2,1)}, /*index=5*/bf16[15...) while((s32[]{:T(128)}, f32[4,384,256]{1,2,0:T(8,128)}, ...), condition=%wide.region_6.7_spmd.clone.clone, body=%wide.region_0.6_spmd.clone.clone.sunk | while | flops 246117120 | bytes 38572464 | solution.py:117
  41.8 27.9 %conditional.4 = ((f32[4,384,256]{1,2,0:T(8,128)}, f32[4,4,384]{2,1,0:T(4,128)})) conditional(s32[]{:T(128)} %convert_element_type.76, (f32[4,384,256]{1,2,0:T(8,128)}, f32[4,4,384]{2,1,0:T(4,128)}) %tuple.53, (s32[]{:T(128)}, bf16[1536,256]{0,1:T(8,128)(2,1)}, s32[]{:T(128)}, bf16[1536,256]{0,1:T(8,128)(2,1)}, bf16[384,4,64]{0,2,1:T(8,128)(2,1)}, ...), branch_computations={%region_1.0_spmd, %region_2.5_spmd} | conditional | flops 246117120 | bytes 38570716 | solution.py:115
  43.7 4.3 %fusion.15 = (f32[4,384]{1,0:T(4,128)S(1)}, f32[4,384,384]{1,2,0:T(8,128)S(1)}, f32[4,384,384]{2,1,0:T(8,128)}) fusion(f32[4,384]{1,0:T(4,128)S(1)} %convert_bitcast_fusion, pred[384,384]{0,1:T(8,128)(4,1)S(1)} %broadcast_compare_fusion, bf16[384,4,64]{0,2,1:T(8,128)(2,1)S(1)} %bitcast.92, bf16[384,4,64]{0,2,1:T(8,128)(2,1)} %get-tuple-element.177), kind=kOutput, calls=%fused_computation.33 | convolution fusion | flops 81984000 | bytes 5271552 | tf_op jit(solution)/shard_map/while/body/eval_jaxpr/cond/branch_1_fun/qhd,khd->hqk/dot_general | solution.py:63
  48.0 14.0 %fusion.2 = f32[4,384,3,128]{1,2,3,0:T(4,128)S(1)} fusion(f32[4,384,3,128]{1,3,2,0:T(8,128)S(1)} %bitcast.88), kind=kOutput, calls=%fused_computation.5 | output fusion | flops 74907648 | bytes 4718592 | tf_op jit(solution)/shard_map/reduce-window
  62.9 1.4 copy-done
  64.3 3.6 fusion.8
  71.4 1.6 fusion.22
  75.2 4.7 %all-to-all-start = ((bf16[8,48,256]{2,1,0:T(8,128)(2,1)}), bf16[8,48,256]{2,1,0:T(8,128)(2,1)S(1)}, u32[]{:S(2)}, u32[]{:S(2)}) async-start(bf16[8,48,256]{2,1,0:T(8,128)(2,1)} %multiply_convert_fusion.2), calls=%async_computation | async-start | bytes 393216 | tf_op jit(solution)/shard_map/all_to_all | solution.py:129
  81.5 12.2 %all-to-all-done = bf16[8,48,256]{2,1,0:T(8,128)(2,1)S(1)} async-done(((bf16[8,48,256]{2,1,0:T(8,128)(2,1)}), bf16[8,48,256]{2,1,0:T(8,128)(2,1)S(1)}, u32[]{:S(2)}, u32[]{:S(2)}) %all-to-all-start) | async-done | bytes 196640 | tf_op jit(solution)/shard_map/all_to_all | solution.py:129
  93.7 4.2 %all-gather.3.cloned.1.call-done = bf16[2048,2048]{1,0:T(8,128)(2,1)} async-done(((bf16[256,2048]{1,0:T(8,128)(2,1)}), bf16[2048,2048]{1,0:T(8,128)(2,1)}) %all-gather.3.cloned.1.call-update) | async-done | bytes 8388624 | tf_op jit(solution)/shard_map/all_gather | solution.py:132
  97.9 5.1 %multiply_reduce_fusion.1 = (f32[48]{0:T(128)S(1)}, f32[48,2048]{1,0:T(8,128)S(1)}) fusion(bf16[48,2048]{1,0:T(8,128)(2,1)S(1)} %bitcast.94, bf16[2048,2048]{1,0:T(8,128)(2,1)} %all-gather.3.cloned.1.call-done, bf16[48,2048]{1,0:T(8,128)(2,1)S(1)} %copy-done.1), kind=kOutput, calls=%fused_computation.54 | convolution fusion | flops 403242944 | bytes 9175232 | tf_op jit(solution)/shard_map/dot_general | solution.py:130
  103.1 1.1 gather_fusion
  104.4 86.9 %all_to_all.26 = bf16[4,1,48,2048]{3,2,1,0:T(8,128)(2,1)} all-to-all(bf16[4,1,48,2048]{3,2,1,0:T(8,128)(2,1)S(1)} %broadcast_select_fusion), channel_id=1, replica_groups=mesh['sp'=4,'tp'=8] {'sp'}, dimensions={0} | all-to-all | bytes 1572864 | tf_op jit(solution)/shard_map/all_to_all | solution.py:143
  191.4 63.5 %all-gather.5.cloned.1.call-done = bf16[32,1,48,2048]{3,2,1,0:T(8,128)(2,1)} async-done(((bf16[4,1,48,2048]{3,2,1,0:T(8,128)(2,1)}), bf16[32,1,48,2048]{3,2,1,0:T(8,128)(2,1)}) %all-gather.5.cloned.1.call-update) | async-done | bytes 6291472 | tf_op jit(solution)/shard_map/all_gather | solution.py:150
  254.9 10.0 %fusion.18 = f32[1536,896]{1,0:T(8,128)S(1)} fusion(bf16[1536,2048]{1,0:T(8,128)(2,1)} %bitcast.101, bf16[1,2048,896]{2,1,0:T(8,128)(2,1)} %param.25), kind=kOutput, calls=%fused_computation.38 | convolution fusion | flops 5637144576 | bytes 15466496 | tf_op jit(solution)/shard_map/dot_general | solution.py:14
  264.9 7.1 %multiply_convert_fusion = bf16[1536,896]{1,0:T(8,128)(2,1)S(1)} fusion(f32[1536,896]{1,0:T(8,128)S(1)} %fusion.18, bf16[1536,2048]{1,0:T(8,128)(2,1)S(1)} %bitcast.102, bf16[1,2048,896]{2,1,0:T(8,128)(2,1)S(1)} %copy-done.9), kind=kOutput, calls=%fused_computation.35 | convolution fusion | flops 5645402112 | bytes 18219008 | tf_op jit(solution)/shard_map/dot_general | solution.py:15
  272.0 8.7 %convert_bitcast_fusion.1 = bf16[32,1,48,2048]{3,2,0,1:T(8,128)(2,1)} fusion(bf16[32,48,896]{2,1,0:T(8,128)(2,1)S(1)} %bitcast.103, bf16[1,896,2048]{2,1,0:T(8,128)(2,1)S(1)} %copy-done.10), kind=kOutput, calls=%fused_computation.34 | convolution fusion | flops 5640290304 | bytes 12713984 | tf_op jit(solution)/shard_map/dot_general | solution.py:17
  280.8 68.5 %reduce-scatter.2.cloned.1.call-done = bf16[4,1,48,2048]{3,2,0,1:T(8,128)(2,1)} async-done(((bf16[32,1,48,2048]{3,2,0,1:T(8,128)(2,1)}), bf16[4,1,48,2048]{3,2,0,1:T(8,128)(2,1)}) %reduce-scatter.2.cloned.1.call-update) | async-done | bytes 786448 | tf_op jit(solution)/shard_map/reduce_scatter | solution.py:160
  349.3 3.7 all-to-all-start.2
  353.5 8.6 %all-to-all-done.2 = bf16[4,1,48,2048]{3,2,1,0:T(8,128)(2,1)S(1)} async-done(((bf16[4,1,48,2048]{3,2,1,0:T(8,128)(2,1)}), bf16[4,1,48,2048]{3,2,1,0:T(8,128)(2,1)S(1)}, u32[]{:S(2)}, u32[]{:S(2)}) %all-to-all-start.2) | async-done | bytes 786464 | tf_op jit(solution)/shard_map/all_to_all | solution.py:161
  363.2 2.1 multiply_reduce_fusion
  (94 shorter events, 17.8 us)
Async XLA Ops:
  6.5 19.3 %copy-start.2 = (bf16[384,256]{1,0:T(8,128)(2,1)S(1)}, bf16[384,256]{1,0:T(8,128)(2,1)}, u32[]{:S(2)}) copy-start(bf16[384,256]{1,0:T(8,128)(2,1)} %param.18) | copy-start | bytes 589828
  6.5 19.5 %copy-start.3 = (bf16[384,256]{1,0:T(8,128)(2,1)S(1)}, bf16[384,256]{1,0:T(8,128)(2,1)}, u32[]{:S(2)}) copy-start(bf16[384,256]{1,0:T(8,128)(2,1)} %param.17) | copy-start | bytes 589828
  6.5 91.4 %all-gather.3.cloned.1.call-start = ((), (), s32[]{:S(2)}) async-start(), calls=%async_computation.4 | async-start | bytes 9437184 | tf_op jit(solution)/shard_map/all_gather | solution.py:132
  62.6 1.7 copy-start
  71.4 3.0 copy-start.6
  73.1 7.0 %copy-start.5 = (s32[48,2]{0,1:T(2,128)S(1)}, s32[48,2]{0,1:T(2,128)}, u32[]{:S(2)}) copy-start(s32[48,2]{0,1:T(2,128)} %param.28) | copy-start | bytes 1156
  73.3 24.6 %copy-start.1 = (bf16[48,2048]{1,0:T(8,128)(2,1)S(1)}, bf16[48,2048]{1,0:T(8,128)(2,1)}, u32[]{:S(2)}) copy-start(bf16[48,2048]{1,0:T(8,128)(2,1)} %param.23) | copy-start | bytes 589828
  75.2 18.4 %all-to-all-start = ((bf16[8,48,256]{2,1,0:T(8,128)(2,1)}), bf16[8,48,256]{2,1,0:T(8,128)(2,1)S(1)}, u32[]{:S(2)}, u32[]{:S(2)}) async-start(bf16[8,48,256]{2,1,0:T(8,128)(2,1)} %multiply_convert_fusion.2), calls=%async_computation | async-start | bytes 393216 | tf_op jit(solution)/shard_map/all_to_all | solution.py:129
  80.0 174.9 %all-gather.5.cloned.1.call-start = ((), (), s32[]{:S(2)}) async-start(), calls=%async_computation.5 | async-start | bytes 7077888 | tf_op jit(solution)/shard_map/all_gather | solution.py:150
  97.9 5.1 %copy-start.4 = (f32[2048]{0:T(1024)S(1)}, f32[2048]{0:T(1024)}, u32[]{:S(2)}) copy-start(f32[2048]{0:T(1024)} %param.24) | copy-start | bytes 24580
  191.3 158.0 %reduce-scatter.2.cloned.1.call-start = ((), (), s32[]{:S(2)}) async-start(), calls=%async_computation.6 | async-start | bytes 7077888 | tf_op jit(solution)/shard_map/reduce_scatter | solution.py:160
  254.9 10.0 %copy-start.8 = (bf16[32,1,48,2048]{3,2,1,0:T(8,128)(2,1)S(1)}, bf16[32,1,48,2048]{3,2,1,0:T(8,128)(2,1)}, u32[]{:S(2)}) copy-start(bf16[32,1,48,2048]{3,2,1,0:T(8,128)(2,1)} %all-gather.5.cloned.1.call-done) | copy-start | bytes 18874372
  254.9 10.0 %copy-start.9 = (bf16[1,2048,896]{2,1,0:T(8,128)(2,1)S(1)}, bf16[1,2048,896]{2,1,0:T(8,128)(2,1)}, u32[]{:S(2)}) copy-start(bf16[1,2048,896]{2,1,0:T(8,128)(2,1)} %param.26) | copy-start | bytes 11010052
  264.9 7.1 %copy-start.10 = (bf16[1,896,2048]{2,1,0:T(8,128)(2,1)S(1)}, bf16[1,896,2048]{2,1,0:T(8,128)(2,1)}, u32[]{:S(2)}) copy-start(bf16[1,896,2048]{2,1,0:T(8,128)(2,1)} %param.27) | copy-start | bytes 11010052
  280.8 72.6 %copy-start.7 = (f32[48,2]{0,1:T(2,128)S(1)}, f32[48,2]{0,1:T(2,128)}, u32[]{:S(2)}) copy-start(f32[48,2]{0,1:T(2,128)} %param.29) | copy-start | bytes 1156
  349.3 12.8 %all-to-all-start.2 = ((bf16[4,1,48,2048]{3,2,1,0:T(8,128)(2,1)}), bf16[4,1,48,2048]{3,2,1,0:T(8,128)(2,1)S(1)}, u32[]{:S(2)}, u32[]{:S(2)}) async-start(bf16[4,1,48,2048]{3,2,1,0:T(8,128)(2,1)} %bitcast.96), calls=%async_computation.3 | async-start | bytes 1572864 | tf_op jit(solution)/shard_map/all_to_all | solution.py:161
Sparse Core Ops, SparseCore 0:
  8.9 88.9 all-gather.2
  191.4 63.4 all-gather.4
  280.9 68.3 reduce-scatter.1
